TPU v7x, 32 devices: a whole 2x2x4 slice. The times are simulated.
32 devices in a mesh: sp: 16 (over z, y, core), tp: 2 (over x).
Axes of the slice: x: 2, y: 2, z: 4, core: 2. Of those that a mesh axis runs over, the one named last changes fastest.
Arguments:
- latent_tokens: bfloat16 [2048, 2048], P(('sp', 'tp')), may hold values from -6 to 6
- context_tokens: bfloat16 [512, 2048], P('sp'), may hold values from -6 to 6
- cond: float32 [2048], replicated, may hold values from -6 to 6
- ctx_cond: float32 [2048], replicated, may hold values from -6 to 6
- mod_shift: bfloat16 [2048, 2048], P('sp', 'tp'), may hold values from -0.125 to 0.125
- mod_scale: bfloat16 [2048, 2048], P('sp', 'tp'), may hold values from -0.125 to 0.125
- mod_gate: bfloat16 [2048, 2048], P('sp', 'tp'), may hold values from -0.125 to 0.125
- norm_gain: float32 [2048], replicated, may hold values from 0.1 to 1.9
- w_query: bfloat16 [2048, 1536], P(None, 'tp'), may hold values from -0.125 to 0.125
- query_gain: float32 [96], replicated, may hold values from 0.8 to 2
- w_down_kv: bfloat16 [2048, 256], replicated, may hold values from -0.125 to 0.125
- w_rope_key: bfloat16 [2048, 32], replicated, may hold values from -0.125 to 0.125
- kv_gain: float32 [256], replicated, may hold values from 0.1 to 1.9
- w_up_kv: bfloat16 [2, 256, 1024], P(None, None, 'tp'), may hold values from -0.375 to 0.375
- key_gain: float32 [96], replicated, may hold values from 0.8 to 2
- ctx_lift: float32 [16], P('tp'), may hold values from 1.5 to 220
- w_output: bfloat16 [1024, 2048], P('tp'), may hold values from -0.1875 to 0.1875
Outputs:
- updated: bfloat16 [2048, 2048], P(('sp', 'tp'))
All inputs are finite; a program needn't handle non-finite values.
Results may differ from a plain program's by a relative error of at most 0.007.
Values may be sent and summed in bfloat16 or wider, within the bound.
A program may use at most 64 MiB of HBM per device.

v0:
```python
import jax
import jax.numpy as jnp
from jax import lax
from jax.sharding import PartitionSpec as P

HD = 64
ROPE = 32
QK = 96
GRID_W = 64


EPS = 1e-06
THETA = 10000.0


def rms_normed(values, gain_vector):
    values = values.astype(jnp.float32)
    inv_root = lax.rsqrt(jnp.mean(values * values, axis=-1, keepdims=True) + EPS)
    return values * inv_root * gain_vector


def grid_angles(position, width):
    freq_count = width // 4
    inverse = THETA ** (-jnp.arange(freq_count, dtype=jnp.float32) / freq_count)
    row_index = (position // GRID_W).astype(jnp.float32)
    col_index = (position % GRID_W).astype(jnp.float32)
    return jnp.concatenate([row_index[:, None] * inverse, col_index[:, None] * inverse], axis=-1)


def rotate_tail(head_rows, angle, plain):
    tail = head_rows[..., plain:]
    half_width = tail.shape[-1] // 2
    cosine = jnp.cos(angle)[:, None, :]
    sine_val = jnp.sin(angle)[:, None, :]
    front_half = tail[..., :half_width]
    back_half = tail[..., half_width:]
    return jnp.concatenate(
        [
            head_rows[..., :plain],
            front_half * cosine - back_half * sine_val,
            back_half * cosine + front_half * sine_val,
        ],
        axis=-1,
    )


def modulation(signal, weight):
    return jnp.dot(signal, weight.astype(jnp.float32), precision=lax.Precision.HIGHEST)


def compress(hidden, w_down_kv, w_rope_key, kv_gain):
    latent = rms_normed(jnp.dot(hidden, w_down_kv, preferred_element_type=jnp.float32), kv_gain)
    rope_key = jnp.dot(hidden, w_rope_key, preferred_element_type=jnp.float32)
    return (latent.astype(jnp.bfloat16), rope_key.astype(jnp.bfloat16))


def expand(latent, rope_key, w_up_kv, key_gain, angle):
    row_count = latent.shape[0]
    head_count = w_up_kv.shape[2] // HD
    key_plain = jnp.dot(latent, w_up_kv[0], preferred_element_type=jnp.float32).reshape(
        row_count, head_count, HD
    )
    shared = jnp.broadcast_to(
        rope_key.astype(jnp.float32)[:, None, :], (row_count, head_count, ROPE)
    )
    keys = rms_normed(jnp.concatenate([key_plain, shared], axis=-1), key_gain)
    if angle is not None:
        keys = rotate_tail(keys, angle, HD)
    values = jnp.dot(latent, w_up_kv[1], preferred_element_type=jnp.float32).astype(jnp.bfloat16)
    return (keys.astype(jnp.bfloat16), values.reshape(row_count, head_count, HD))


def absorb(carry, query_heads, keys, values, lift):
    highest, total, mixed = carry
    scores = (
        jnp.einsum("qhd,khd->hqk", query_heads, keys, preferred_element_type=jnp.float32)
        * QK ** (-0.5)
        + lift
    )
    new_high = jnp.maximum(highest, jnp.max(scores, axis=-1))
    weights = jnp.exp(scores - new_high[:, :, None])
    factor = jnp.exp(highest - new_high)
    total = total * factor + jnp.sum(weights, axis=-1)
    update = jnp.einsum(
        "hqk,khd->qhd", weights.astype(jnp.bfloat16), values, preferred_element_type=jnp.float32
    )
    mixed = mixed * jnp.transpose(factor)[:, :, None] + update
    return (new_high, total, mixed)


def local(
    latent_tokens,
    context_tokens,
    cond,
    ctx_cond,
    mod_shift,
    mod_scale,
    mod_gate,
    norm_gain,
    w_query,
    query_gain,
    w_down_kv,
    w_rope_key,
    kv_gain,
    w_up_kv,
    key_gain,
    ctx_lift,
    w_output,
):
    tp_count = lax.axis_size("tp")
    sp_index = lax.axis_index("sp")
    tp_index = lax.axis_index("tp")
    piece_rows = mod_shift.shape[0]
    piece_cols = mod_shift.shape[1]
    own_start = sp_index * piece_rows
    lat_signal = jax.nn.silu(lax.dynamic_slice_in_dim(cond, own_start, piece_rows, 0))
    ctx_signal = jax.nn.silu(lax.dynamic_slice_in_dim(ctx_cond, own_start, piece_rows, 0))
    both_signal = jnp.stack([lat_signal, ctx_signal])
    shift_part = modulation(both_signal, mod_shift)
    scale_part = modulation(both_signal, mod_scale)
    gate_part = modulation(lat_signal[None, :], mod_gate)
    full_cols = piece_cols * tp_count

    def widen(part):
        zeros = jnp.zeros((part.shape[0], full_cols), jnp.float32)
        return lax.dynamic_update_slice_in_dim(zeros, part, tp_index * piece_cols, 1)

    shift_vec, scale_vec, gate_vec = lax.psum(
        (widen(shift_part), widen(scale_part), widen(gate_part)), ("sp", "tp")
    )
    hidden_lat = (
        rms_normed(latent_tokens, norm_gain) * (1.0 + scale_vec[0]) + shift_vec[0]
    ).astype(jnp.bfloat16)
    ctx_rows = lax.all_gather(context_tokens, "sp", axis=0, tiled=True)
    ctx_hidden = (rms_normed(ctx_rows, norm_gain) * (1.0 + scale_vec[1]) + shift_vec[1]).astype(
        jnp.bfloat16
    )
    ctx_latent, ctx_rope = compress(ctx_hidden, w_down_kv, w_rope_key, kv_gain)
    ctx_keys, ctx_values = expand(ctx_latent, ctx_rope, w_up_kv, key_gain, None)
    head_count = ctx_lift.shape[0]
    local_rows = latent_tokens.shape[0]
    group_rows = local_rows * tp_count
    group_start = sp_index * group_rows
    qk_width = head_count * QK
    piece = lax.all_gather(hidden_lat, "tp", axis=0, tiled=True)
    row_count = piece.shape[0]
    position = group_start + jnp.arange(row_count, dtype=jnp.int32)
    raw = jnp.dot(piece, w_query, preferred_element_type=jnp.float32).reshape(
        row_count, head_count, QK
    )
    turned = rotate_tail(rms_normed(raw, query_gain), grid_angles(position, ROPE), HD)
    queries = turned.astype(jnp.bfloat16).reshape(row_count, qk_width)
    own_latent, own_rope = compress(hidden_lat, w_down_kv, w_rope_key, kv_gain)
    query_heads = queries.reshape(group_rows, head_count, QK)
    start_carry = (
        jnp.full((head_count, group_rows), -1e30, jnp.float32),
        jnp.zeros((head_count, group_rows), jnp.float32),
        jnp.zeros((group_rows, head_count, HD), jnp.float32),
    )
    carry = absorb(start_carry, query_heads, ctx_keys, ctx_values, ctx_lift[:, None, None])
    pieces = (
        lax.all_gather(own_latent, ("sp", "tp"), axis=0, tiled=True),
        lax.all_gather(own_rope, ("sp", "tp"), axis=0, tiled=True),
    )
    row_count = pieces[0].shape[0]
    position = jnp.arange(row_count, dtype=jnp.int32)
    keys, values = expand(pieces[0], pieces[1], w_up_kv, key_gain, grid_angles(position, ROPE))
    carry = absorb(carry, query_heads, keys, values, 0.0)
    highest, total, mixed = carry
    attended = (
        (mixed / jnp.transpose(total)[:, :, None])
        .astype(jnp.bfloat16)
        .reshape(group_rows, head_count * HD)
    )
    out = lax.psum_scatter(
        jnp.dot(attended, w_output, preferred_element_type=jnp.float32).astype(jnp.bfloat16),
        "tp",
        scatter_dimension=0,
        tiled=True,
    ).astype(jnp.float32)
    return (latent_tokens.astype(jnp.float32) + gate_vec[0] * out).astype(jnp.bfloat16)


def solution(mesh):
    return jax.shard_map(
        local,
        mesh=mesh,
        in_specs=(
            P(("sp", "tp"), None),
            P("sp", None),
            P(),
            P(),
            P("sp", "tp"),
            P("sp", "tp"),
            P("sp", "tp"),
            P(),
            P(None, "tp"),
            P(),
            P(),
            P(),
            P(),
            P(None, None, "tp"),
            P(),
            P("tp"),
            P("tp", None),
        ),
        out_specs=P(("sp", "tp"), None),
        check_vma=False,
    )
```

profile of v0, /device:TPU:0, one launch (start us, length us, event | category | flops | bytes accessed | tf_op | source)
XLA Modules:
  0.0 198.8 jit_solution(2689586733869971769)
XLA Ops:
  6.6 0.9 fusion.74
  7.5 1.3 fusion.72
  8.8 1.2 convolution_dynamic-update-slice_fusion.1
  10.0 1.2 convolution_dynamic-update-slice_fusion
  11.2 0.3 dynamic_update_slice.12
  11.5 42.3 %all-reduce = (f32[2,2048]{1,0:T(2,128)S(1)}, f32[2,2048]{1,0:T(2,128)S(1)}, f32[2048]{0:T(1024)S(1)}) all-reduce(f32[2,2048]{1,0:T(2,128)S(1)} %convolution_dynamic-update-slice_fusion, f32[2,2048]{1,0:T(2,128)S(1)} %convolution_dynamic-update-slice_fusion.1, ...), channel_id=1, replica_groups=mesh['sp'=16,'tp'=2] {'sp','tp'}, use_global_device_ids=true, to_apply=%region_3.4 | all-reduce | flops 10240 | bytes 81920 | tf_op jit(solution)/shard_map/psum | solution.py:128
  53.8 0.6 slice_add_fusion
  54.4 0.6 fusion.86
  55.0 1.1 fusion.39
  56.2 1.1 fusion.43
  57.3 1.6 multiply_reduce_fusion.5
  59.0 0.7 multiply_convert_fusion.3
  59.7 0.7 all-gather.4.cloned.1.call-update
  60.5 8.1 %all_gather.12 = bf16[128,2048]{1,0:T(8,128)(2,1)} all-gather(bf16[64,2048]{1,0:T(8,128)(2,1)S(1)} %fusion.43), channel_id=1, replica_groups=mesh['sp'=16,'tp'=2] {'tp'}, dimensions={0}, use_global_device_ids=true | all-gather | bytes 786432 | tf_op jit(solution)/shard_map/all_gather | solution.py:145
  68.5 0.6 fusion.71
  69.1 1.7 slice_bitcast_fusion
  70.8 1.8 copy.26
  72.8 2.4 %fusion.87 = f32[128,768]{0,1:T(8,128)S(1)} fusion(bf16[128,2048]{1,0:T(8,128)(2,1)} %all_gather.12, bf16[2048,768]{1,0:T(8,128)(2,1)S(1)} %copy-done), kind=kOutput, calls=%fused_computation.151 | convolution fusion | flops 402653184 | bytes 4063232 | tf_op jit(solution)/shard_map/dot_general | solution.py:148
  75.3 1.5 multiply_multiply_fusion.1
  76.9 66.9 %all-gather = bf16[32,64,32]{1,2,0:T(8,128)(2,1)S(1)} all-gather(bf16[1,64,32]{1,2,0:T(8,128)(2,1)S(1)} %fusion.29), channel_id=1, replica_groups=mesh['sp'=16,'tp'=2] {'sp','tp'}, dimensions={0}, use_global_device_ids=true | all-gather | bytes 135168 | tf_op jit(solution)/shard_map/all_gather | solution.py:163
  143.8 0.9 copy.28
  144.7 1.9 reshape.274
  146.6 1.6 slice.90
  148.3 1.5 subtract_convert_fusion.1
  149.9 1.1 fusion.52
  151.0 2.0 %fusion.31 = f32[2048,8,64]{0,2,1:T(8,128)S(1)} fusion(bf16[8,64,256]{2,1,0:T(8,128)(2,1)S(1)} %bitcast.94, bf16[2048,256]{1,0:T(8,128)(2,1)} %all-gather.6.cloned.1.call-done), kind=kOutput, calls=%fused_computation.48 | convolution fusion | flops 536870912 | bytes 5505024 | tf_op jit(solution)/shard_map/dot_general | solution.py:60
  153.3 0.8 multiply_reduce_fusion.1
  154.1 1.4 multiply_multiply_fusion
  155.6 0.3 slice.89
  156.0 0.9 copy-done.2
  157.0 2.1 %convolution_convert_fusion = bf16[2048,512]{0,1:T(8,128)(2,1)} fusion(bf16[2048,256]{1,0:T(8,128)(2,1)S(1)} %copy-done.2, bf16[2,256,512]{2,1,0:T(8,128)(2,1)S(1)} %copy-done.7), kind=kOutput, calls=%fused_computation.24 | convolution fusion | flops 537919488 | bytes 3407872 | tf_op jit(solution)/shard_map/dot_general | solution.py:69
  159.1 0.3 subtract_convert_fusion
  159.4 4.2 %multiply_reduce_fusion = (f32[8,128]{1,0:T(8,128)S(1)}, f32[8,128,2048]{2,1,0:T(8,128)}) fusion(bf16[2048,8,16]{0,2,1:T(8,128)(2,1)S(1)} %get-tuple-element.11, bf16[2048,8,16]{0,2,1:T(8,128)(2,1)S(1)} %get-tuple-element.10, bf16[2048,8,64]{0,2,1:T(8,128)(2,1)S(1)} %slice.89, bf16[128,8,16]{0,2,1:T(8,128)(2,1)S(1)} %copy-done.17, ...), kind=kOutput, calls=%fused_computation.1 | convolution fusion | flops 416873472 | bytes 11735040 | tf_op jit(solution)/shard_map/qhd,khd->hqk/dot_general | solution.py:76
  163.6 2.1 %fusion.2 = f32[512]{0:T(512)S(1)} fusion(bf16[512,2048]{1,0:T(8,128)(2,1)} %all-gather.4.cloned.1.call-done), kind=kLoop, calls=%fused_computation.9 | loop fusion | flops 3145216 | bytes 2099200 | tf_op jit(solution)/shard_map/reduce_sum | solution.py:18
  165.7 3.1 %multiply_reduce_fusion.3 = (f32[512]{0:T(512)S(1)}, f32[512,256]{0,1:T(8,128)S(1)}) fusion(bf16[2048,256]{1,0:T(8,128)(2,1)} %param.27, bf16[512,2048]{1,0:T(8,128)(2,1)} %all-gather.4.cloned.1.call-done, f32[2048]{0:T(1024)S(1)} %bitcast.103, f32[2048]{0:T(1024)S(1)} %bitcast.101, f32[2048]{0:T(1024)S(1)} %copy-done.20, f32[512]{0:T(512)S(1)} %add_rsqrt_fusion.4), kind=kOutput, calls=%fused_computation.68 | convolution fusion | flops 543424000 | bytes 3698688 | tf_op jit(solution)/shard_map/dot_general | solution.py:52
  168.9 0.4 fusion.47
  169.3 0.4 convolution_convert_fusion.2
  169.7 0.7 copy-done.5
  170.4 1.0 fusion.28
  171.8 0.6 fusion.17
  172.4 0.8 slice-done.1
  173.2 1.6 fusion
  174.9 1.7 fusion.20
  176.6 0.6 fusion.18
  177.2 0.7 fusion.27
  178.1 1.3 convolution_convert_fusion.1
  179.4 11.1 %reduce-scatter.2.cloned.1.call-done = bf16[64,2048]{1,0:T(8,128)(2,1)} async-done(((bf16[128,2048]{1,0:T(8,128)(2,1)}), bf16[64,2048]{1,0:T(8,128)(2,1)}) %reduce-scatter.2.cloned.1.call-update) | async-done | bytes 262160 | tf_op jit(solution)/shard_map/reduce_scatter | solution.py:175
  190.6 1.7 fusion.44
  (85 shorter events, 1.6 us)
Async XLA Ops:
  6.5 66.3 %copy-start = (bf16[2048,768]{1,0:T(8,128)(2,1)S(1)}, bf16[2048,768]{1,0:T(8,128)(2,1)}, u32[]{:S(2)}) copy-start(bf16[2048,768]{1,0:T(8,128)(2,1)} %param.25) | copy-start | bytes 9437188
  6.5 52.4 %copy-start.19 = (f32[256]{0:T(256)S(1)}, f32[256]{0:T(256)}, u32[]{:S(2)}) copy-start(f32[256]{0:T(256)} %param.29) | copy-start | bytes 3076
  6.5 66.1 %copy-start.11 = (bf16[2048,32]{0,1:T(8,128)(2,1)S(1)}, bf16[2048,32]{0,1:T(8,128)(2,1)}, u32[]{:S(2)}) copy-start(bf16[2048,32]{0,1:T(8,128)(2,1)} %param.28) | copy-start | bytes 393220
  6.5 144.4 %all-gather.6.cloned.1.call-start = ((), (), s32[]{:S(2)}) async-start(), calls=%async_computation.2 | async-start | bytes 1081344 | tf_op jit(solution)/shard_map/all_gather | solution.py:162
  59.7 103.9 %all-gather.4.cloned.1.call-start = ((), (), s32[]{:S(2)}) async-start(), calls=%async_computation.1 | async-start | bytes 2228224 | tf_op jit(solution)/shard_map/all_gather | solution.py:134
  60.4 130.2 %reduce-scatter.2.cloned.1.call-start = ((), (), s32[]{:S(2)}) async-start(), calls=%async_computation.3 | async-start | bytes 786432 | tf_op jit(solution)/shard_map/reduce_scatter | solution.py:175
  72.6 4.2 %copy-start.25 = (f32[128]{0:T(128)S(1)}, f32[128]{0:T(128)}, u32[]{:S(2)}) copy-start(f32[128]{0:T(128)} %get-tuple-element.37) | copy-start | bytes 1540
  72.6 4.2 %copy-start.26 = (f32[128]{0:T(128)S(1)}, f32[128]{0:T(128)}, u32[]{:S(2)}) copy-start(f32[128]{0:T(128)} %get-tuple-element.38) | copy-start | bytes 1540
  72.8 78.2 %copy-start.3 = (bf16[512,256]{1,0:T(8,128)(2,1)S(1)}, bf16[512,256]{1,0:T(8,128)(2,1)}, u32[]{:S(2)}) copy-start(bf16[512,256]{1,0:T(8,128)(2,1)} %copy.26) | copy-start | bytes 786436
  151.0 2.0 %copy-start.9 = (f32[2048,32]{0,1:T(8,128)S(1)}, f32[2048,32]{0,1:T(8,128)}, u32[]{:S(2)}) copy-start(f32[2048,32]{0,1:T(8,128)} %reshape.274) | copy-start | bytes 786436
  153.3 0.9 copy-start.23
  155.6 1.2 copy-start.2
  155.6 1.4 copy-start.7
  155.6 3.4 %copy-start.10 = (f32[2048,16]{0,1:T(8,128)S(1)}, f32[2048,16]{0,1:T(8,128)}, u32[]{:S(2)}) copy-start(f32[2048,16]{0,1:T(8,128)} %get-tuple-element.15) | copy-start | bytes 393220
  157.0 2.4 %copy-start.13 = (bf16[128,8,64]{0,2,1:T(8,128)(2,1)S(1)}, bf16[128,8,64]{0,2,1:T(8,128)(2,1)}, u32[]{:S(2)}) copy-start(bf16[128,8,64]{0,2,1:T(8,128)(2,1)} %slice.90) | copy-start | bytes 393220
  157.0 2.4 %copy-start.15 = (bf16[128,8,16]{0,2,1:T(8,128)(2,1)S(1)}, bf16[128,8,16]{0,2,1:T(8,128)(2,1)}, u32[]{:S(2)}) copy-start(bf16[128,8,16]{0,2,1:T(8,128)(2,1)} %get-tuple-element.12) | copy-start | bytes 98308
  157.0 2.4 %copy-start.17 = (bf16[128,8,16]{0,2,1:T(8,128)(2,1)S(1)}, bf16[128,8,16]{0,2,1:T(8,128)(2,1)}, u32[]{:S(2)}) copy-start(bf16[128,8,16]{0,2,1:T(8,128)(2,1)} %get-tuple-element.13) | copy-start | bytes 98308
  159.4 6.3 %copy-start.20 = (f32[2048]{0:T(1024)S(1)}, f32[2048]{0:T(1024)}, u32[]{:S(2)}) copy-start(f32[2048]{0:T(1024)} %param.24) | copy-start | bytes 24580
  159.4 6.3 %copy-start.21 = (f32[1,2048]{1,0:T(1,128)S(1)}, f32[1,2048]{1,0:T(1,128)}, u32[]{:S(2)}) copy-start(f32[1,2048]{1,0:T(1,128)} %get-tuple-element.16) | copy-start | bytes 24580
  159.4 6.3 %copy-start.22 = (f32[1,2048]{1,0:T(1,128)S(1)}, f32[1,2048]{1,0:T(1,128)}, u32[]{:S(2)}) copy-start(f32[1,2048]{1,0:T(1,128)} %get-tuple-element.18) | copy-start | bytes 24580
  165.7 3.5 %copy-start.8 = (bf16[2,256,512]{2,1,0:T(8,128)(2,1)S(1)}, bf16[2,256,512]{2,1,0:T(8,128)(2,1)}, u32[]{:S(2)}) copy-start(bf16[2,256,512]{2,1,0:T(8,128)(2,1)} %param.30) | copy-start | bytes 1572868
  168.8 1.6 copy-start.5
  168.8 1.6 copy-start.12
  168.9 3.6 %slice-start = ((s8[8388608]{0:T(1024)(128)(4,1)}), s8[4194304]{0:T(1024)(128)(4,1)S(1)}, s32[]{:S(2)}) async-start(s8[8388608]{0:T(1024)(128)(4,1)} %bitcast.89), calls=%async_computation.4 | async-start | bytes 8388608
  170.4 1.3 copy-start.14
  170.4 1.3 copy-start.16
  170.4 1.3 copy-start.18
  170.4 1.3 copy-start.24
  170.4 2.8 %slice-start.1 = ((s8[8388608]{0:T(1024)(128)(4,1)}), s8[4194304]{0:T(1024)(128)(4,1)S(1)}, s32[]{:S(2)}) async-start(s8[8388608]{0:T(1024)(128)(4,1)} %bitcast.89), calls=%async_computation.5 | async-start | bytes 8388608
  173.2 1.6 copy-start.1
  176.6 1.6 copy-start.6
  177.2 13.3 %copy-start.4 = (bf16[64,2048]{1,0:T(8,128)(2,1)S(1)}, bf16[64,2048]{1,0:T(8,128)(2,1)}, u32[]{:S(2)}) copy-start(bf16[64,2048]{1,0:T(8,128)(2,1)} %param.17) | copy-start | bytes 786436
Sparse Core Ops, SparseCore 0:
  59.8 53.6 all-gather.5
  115.7 40.5 all-gather.3
  179.6 10.9 reduce-scatter.1
where the time goes:
time: 200 us; the launch traced here: 199 us
  blocking collectives  117 us (58%)
  matrix products  25.4 us (13%)
  other arithmetic  18.4 us (9%)
  between operations  13.6 us (7%)
  local copies, waits for them, and re-layouts  12.3 us (6%)
  waiting for transfers between devices  11.9 us (6%)
    all_gather x1, blocking collectives, local(): lax.all_gather(own_rope, ('sp', 'tp'), axis=0, tiled=True)  66.9 us
    psum x1, blocking collectives, local(): lax.psum((widen(shift_part), widen(scale_part), widen(gate_part)), ('sp',...  42.3 us
    reduce_scatter x1, waiting for transfers between devices, local(): lax.psum_scatter(jnp.dot(attended, w_output, preferred_element_type=jnp.f...  11.1 us
    all_gather x1, blocking collectives, local(): piece = lax.all_gather(hidden_lat, 'tp', axis=0, tiled=True)  8.06 us
    dot_general x2, matrix products, absorb(): jnp.einsum('qhd,khd->hqk', query_heads, keys, preferred_element_type=jnp....  4.84 us
    dot_general x2, matrix products, compress(): jnp.dot(hidden, w_down_kv, preferred_element_type=jnp.float32)  4.71 us
    reduce_sum x5, other arithmetic, rms_normed(): jnp.mean(values * values, axis=-1, keepdims=True) + EPS  4.24 us
  transfers between devices with their start and end apart: 3, of which 1 were waited for; matrix products, arithmetic and copies ran while one was open for 14% of the time, Pallas kernels for 0%

commit v1 on v0

v1 whole, which is shorter than its diff:
```python
import functools

import jax
import jax.numpy as jnp
import numpy as np
from jax import lax
from jax.experimental import pallas as pl
from jax.experimental.pallas import tpu as pltpu
from jax.sharding import PartitionSpec as P

HD = 64
ROPE = 32
QK = 96
GRID_W = 64
EPS = 1e-06
THETA = 10000.0
LANE = 128
MESH = pl.DeviceIdType.MESH
F32 = jnp.float32
BF16 = jnp.bfloat16

NN = (((1,), (0,)), ((), ()))
NT = (((1,), (1,)), ((), ()))


def dot(a, b, dims=NN):
    return lax.dot_general(a, b, dims, preferred_element_type=F32)


def column(row):
    return jnp.transpose(jnp.broadcast_to(row, (LANE, row.shape[1])))


def kernel(
    sizes,
    tok_ref, ctx_ref, cond_ref, cctx_ref, mshift_ref, mscale_ref, mgate_ref, ngain_ref,
    wq_hbm, qgain_ref, wd_hbm, wr_hbm, kvgain_ref, wup_hbm, kgain_ref, lift_ref, wo_hbm,
    cos_ref, sin_ref,
    out_ref,
    wq, wd, wr, wup, wo, part, rsb, red, mod, tokall, hid, chid, G, H, X, rot, ssr, wkT, Q, att,
    sendb, recvb,
    wsem, tok_s, tok_r, rs_s, rs_r, ag_s, ag_r, gz_s, gz_r, hz_s, hz_r, gy_s, gy_r, hy_s, hy_r,
    gx_s, gx_r, gc_s, gc_r, hc_s, hc_r, ob_s, ob_r,
):
    SP, T, Y, C, q, rows, crows, heads = sizes
    Z = SP // (Y * C)
    ND = SP * T
    D = tok_ref.shape[1]
    group = rows * T
    crp = H.shape[3] - 16
    n_ctx = crows * SP
    n_lat = group * SP
    N = n_ctx + n_lat
    sp = lax.axis_index("sp")
    tp = lax.axis_index("tp")
    c = lax.rem(sp, C)
    y = lax.rem(sp // C, Y)
    z = sp // (C * Y)
    flat = sp * T + tp

    barrier = pltpu.get_barrier_semaphore()

    def greet(k, _):
        other = lax.rem(flat + k, ND)
        pl.semaphore_signal(barrier, inc=1, device_id=(other // T, lax.rem(other, T)), device_id_type=MESH)
        return 0

    lax.fori_loop(1, ND, greet, 0)

    wcopies = [
        pltpu.make_async_copy(src, dst, wsem.at[i])
        for i, (src, dst) in enumerate(((wq_hbm, wq), (wd_hbm, wd), (wr_hbm, wr), (wup_hbm, wup), (wo_hbm, wo)))
    ]
    for cp in wcopies:
        cp.start()

    sig_l = cond_ref[pl.ds(sp, 1), :]
    sig_l = column(sig_l * jax.nn.sigmoid(sig_l))
    sig_c = cctx_ref[pl.ds(sp, 1), :]
    sig_c = column(sig_c * jax.nn.sigmoid(sig_c))
    pcols = mshift_ref.shape[1] // LANE

    def put(v, j, val):
        i = v * pcols + j
        part[i // q, i % q : i % q + 1, :] = val

    for j in range(pcols):
        cols = slice(j * LANE, (j + 1) * LANE)
        w = mshift_ref[:, cols].astype(F32)
        put(0, j, jnp.sum(w * sig_l, axis=0, keepdims=True))
        put(1, j, jnp.sum(w * sig_c, axis=0, keepdims=True))
        w = mscale_ref[:, cols].astype(F32)
        put(2, j, jnp.sum(w * sig_l, axis=0, keepdims=True))
        put(3, j, jnp.sum(w * sig_c, axis=0, keepdims=True))
        w = mgate_ref[:, cols].astype(F32)
        put(4, j, jnp.sum(w * sig_l, axis=0, keepdims=True))
    for i in range(5 * pcols, SP * q):
        part[i // q, i % q : i % q + 1, :] = jnp.zeros((1, LANE), F32)

    pl.semaphore_wait(barrier, ND - 1)

    def rs_copy(k):
        other = lax.rem(sp + k, SP)
        return pltpu.make_async_remote_copy(
            src_ref=part.at[other], dst_ref=rsb.at[sp], send_sem=rs_s.at[k - 1], recv_sem=rs_r.at[k - 1],
            device_id=(other, tp), device_id_type=MESH)

    def rs_start(k, _):
        rs_copy(k).start()
        return 0

    lax.fori_loop(1, SP, rs_start, 0)

    def tp_copy(k, src, dst, s, r):
        return pltpu.make_async_remote_copy(
            src_ref=src, dst_ref=dst, send_sem=s.at[k - 1], recv_sem=r.at[k - 1],
            device_id=(sp, lax.rem(tp + k, T)), device_id_type=MESH)

    tok_copies = [tp_copy(k, tok_ref, tokall.at[tp], tok_s, tok_r) for k in range(1, T)]
    for cp in tok_copies:
        cp.start()

    rsb[sp] = part[sp]
    tokall[tp] = tok_ref[...]

    def rs_wait(k, _):
        rs_copy(k).wait()
        return 0

    lax.fori_loop(1, SP, rs_wait, 0)
    total = rsb[0]
    for i in range(1, SP):
        total = total + rsb[i]
    red[...] = total

    def ag_copy(k):
        other = lax.rem(flat + k, ND)
        return pltpu.make_async_remote_copy(
            src_ref=red, dst_ref=mod.at[tp, sp], send_sem=ag_s.at[k - 1], recv_sem=ag_r.at[k - 1],
            device_id=(other // T, lax.rem(other, T)), device_id_type=MESH)

    def ag_start(k, _):
        ag_copy(k).start()
        return 0

    lax.fori_loop(1, ND, ag_start, 0)
    mod[tp, sp] = total

    for cp in wcopies:
        cp.wait()
    wkT[...] = jnp.transpose(wup[0].astype(F32)).astype(BF16)
    kg = column(kgain_ref[...])
    qg = column(qgain_ref[...])
    for cp in tok_copies:
        cp.wait()
    xs = [tokall[t].astype(F32) for t in range(T)]
    invs = [lax.rsqrt(jnp.mean(x * x, axis=1, keepdims=True) + EPS) for x in xs]
    xc = ctx_ref[...].astype(F32)
    invc = lax.rsqrt(jnp.mean(xc * xc, axis=1, keepdims=True) + EPS)

    def ag_wait(k, _):
        ag_copy(k).wait()
        return 0

    lax.fori_loop(1, ND, ag_wait, 0)

    def vec(v, col):
        i = v * pcols + col % pcols
        return mod[col // pcols, i // q, i % q : i % q + 1, :]

    for j in range(D // LANE):
        cols = slice(j * LANE, (j + 1) * LANE)
        g = ngain_ref[:, cols]
        a, b = 1.0 + vec(2, j), vec(0, j)
        for t in range(T):
            hid[t, :, cols] = (tokall[t, :, cols].astype(F32) * invs[t] * g * a + b).astype(BF16)
        a, b = 1.0 + vec(3, j), vec(1, j)
        chid[:, cols] = (ctx_ref[:, cols].astype(F32) * invc * g * a + b).astype(BF16)

    def squeeze(h):
        raw = dot(h, wd[...])
        return raw * lax.rsqrt(jnp.mean(raw * raw, axis=1, keepdims=True) + EPS) * kvgain_ref[...]

    lane = lax.broadcasted_iota(jnp.int32, (ROPE, LANE), 1)
    H[z, y, c, 0:crows] = squeeze(chid[...]).astype(BF16)
    cr = dot(chid[...], wr[...])
    crt = jnp.transpose(jnp.concatenate([cr] * (LANE // crows), axis=0))
    clo = lax.rem(sp, LANE // crows) * crows
    crt = jnp.where((lane >= clo) & (lane < clo + crows), crt, 0.0).astype(BF16)
    H[z, y, c, crp : crp + 16] = jnp.concatenate([crt[:16], crt[16:]], axis=1)
    hid_all = hid[...].reshape(group, D)
    G[z, y, c, tp, 0:rows] = squeeze(hid[tp]).astype(BF16)
    lr = jnp.transpose(dot(hid_all, wr[...]))
    llo = tp * rows
    lr = jnp.where((lane >= llo) & (lane < llo + rows), lr, 0.0).astype(BF16)
    G[z, y, c, tp, rows : rows + 16] = jnp.concatenate([lr[:16], lr[16:]], axis=1)

    def at(zz, yy, cc):
        return (zz * Y + yy) * C + cc

    def remote(src, s, r, dev):
        return pltpu.make_async_remote_copy(
            src_ref=src, dst_ref=src, send_sem=s, recv_sem=r, device_id=dev, device_id_type=MESH)

    zc = []
    for k in range(1, Z):
        dev = (at(lax.rem(z + k, Z), y, c), tp)
        zc.append(remote(G.at[z, y, c, tp], gz_s.at[k - 1], gz_r.at[k - 1], dev))
        zc.append(remote(H.at[z, y, c], hz_s.at[k - 1], hz_r.at[k - 1], dev))
    for cp in zc:
        cp.start()

    raw = dot(hid_all, wq[...])
    rawT = jnp.transpose(raw)
    cosg = cos_ref[:, pl.ds(pl.multiple_of(sp * group, group), group)]
    sing = sin_ref[:, pl.ds(pl.multiple_of(sp * group, group), group)]
    fold = QK ** (-0.5) * 1.4426950408889634
    for h in range(heads):
        u = rawT[h * QK : (h + 1) * QK]
        u = u * (lax.rsqrt(jnp.mean(u * u, axis=0, keepdims=True) + EPS) * fold) * qg[:, :group]
        f, b = u[HD : HD + 16], u[HD + 16 :]
        u = jnp.concatenate([u[:HD], f * cosg - b * sing, b * cosg + f * sing], axis=0)
        Q[h] = jnp.transpose(u).astype(BF16)

    for cp in zc:
        cp.wait()

    ydev = (at(z, Y - 1 - y, c), tp)

    def both(copies):
        for cp in copies:
            cp.start()
        for cp in copies:
            cp.wait()

    def xdev(k):
        return (sp, lax.rem(tp + k, T))

    @pl.when(c == 0)
    def _():
        both([
            remote(G.at[:, y, 0, tp], gy_s.at[0], gy_r.at[0], ydev),
            remote(H.at[:, y, 0], hy_s.at[0], hy_r.at[0], ydev),
        ])
        both([remote(G.at[:, :, 0, tp], gx_s.at[k - 1], gx_r.at[k - 1], xdev(k)) for k in range(1, T)])

    @pl.when(c != 0)
    def _():
        both([remote(G.at[:, y, 1, tp], gx_s.at[k - 1], gx_r.at[k - 1], xdev(k)) for k in range(1, T)])
        both([
            remote(G.at[:, y, 1], gy_s.at[0], gy_r.at[0], ydev),
            remote(H.at[:, y, 1], hy_s.at[0], hy_r.at[0], ydev),
        ])

    cdev = (at(z, y, C - 1 - c), tp)
    both([
        remote(G.at[:, :, c], gc_s.at[0], gc_r.at[0], cdev),
        remote(H.at[:, :, c], hc_s.at[0], hc_r.at[0], cdev),
    ])

    def where_is(s):
        return s // (Y * C), (s // C) % Y, s % C

    step = crows if crows % 16 == 0 else 16
    if crows % 16 == 0:
        for s in range(SP):
            zz, yy, cc = where_is(s)
            X[s * crows : (s + 1) * crows] = H[zz, yy, cc, 0:crows]
    else:
        X[0:n_ctx] = jnp.concatenate(
            [H[where_is(s)][0:16].astype(F32)[:crows] for s in range(SP)], axis=0).astype(BF16)
    per = LANE // crows
    gk = kg[HD:]
    gf, gb = gk[:16], gk[16:]
    for s0 in range(0, SP, per):
        both_half = sum(H[where_is(s)][crp : crp + 16].astype(F32) for s in range(s0, s0 + per))
        f, b = both_half[:, :LANE], both_half[:, LANE:]
        cols = slice(s0 * crows, s0 * crows + LANE)
        ssr[:, cols] = jnp.sum(f * f + b * b, axis=0, keepdims=True)
        rot[0:16, cols] = f * gf
        rot[16:32, cols] = b * gb
    for s in range(SP):
        zz, yy, cc = where_is(s)
        total = 0.0
        for t in range(T):
            lo = n_ctx + s * group + t * rows
            X[lo : lo + rows] = G[zz, yy, cc, t, 0:rows]
            total = total + G[zz, yy, cc, t, rows : rows + 16].astype(F32)
        f, b = total[:, :LANE], total[:, LANE:]
        cols = slice(n_ctx + s * group, n_ctx + (s + 1) * group)
        pos = slice(s * group, (s + 1) * group)
        ssr[:, cols] = jnp.sum(f * f + b * b, axis=0, keepdims=True)
        f, b = f * gf, b * gb
        rot[0:16, cols] = f * cos_ref[:, pos] - b * sin_ref[:, pos]
        rot[16:32, cols] = b * cos_ref[:, pos] + f * sin_ref[:, pos]

    gp = kg[:HD, :1]
    ones = jnp.ones((N, LANE), BF16)
    half = lax.broadcasted_iota(jnp.int32, (group, LANE), 1) < HD

    def pair(p, _):
        lo = pl.multiple_of(p * LANE, LANE)
        kT = dot(wkT[pl.ds(lo, LANE), :], X[...], NT)
        val = jnp.concatenate([dot(X[...], wup[1, :, pl.ds(lo, LANE)]).astype(BF16), ones], axis=1)
        res = []
        for i in range(2):
            kp = kT[i * HD : (i + 1) * HD]
            inv = lax.rsqrt((jnp.sum(kp * kp, axis=0, keepdims=True) + ssr[...]) * (1.0 / QK) + EPS)
            key = jnp.concatenate([kp * gp * inv, rot[...] * inv], axis=0).astype(BF16)
            w = jnp.exp2(dot(Q[2 * p + i], key)).astype(BF16)
            drop = jnp.exp(jnp.full((1, 2 * LANE), -lift_ref[2 * p + i], F32))
            o = dot(w[:, :n_ctx], val[:n_ctx]) + drop * dot(w[:, n_ctx:], val[n_ctx:])
            res.append(o[:, :LANE] / o[:, LANE:])
        att[:, pl.ds(lo, LANE)] = jnp.where(half, res[0], res[1]).astype(BF16)
        return 0

    lax.fori_loop(0, heads // 2, pair, 0)

    for k in range(1, T):
        t = lax.rem(tp + k, T)
        a = att[pl.ds(pl.multiple_of(t * rows, rows), rows), :]
        sendb[k - 1] = dot(a, wo[...]).astype(BF16)
    copies = [tp_copy(k, sendb.at[k - 1], recvb.at[k - 1], ob_s, ob_r) for k in range(1, T)]
    for cp in copies:
        cp.start()
    acc = dot(att[pl.ds(pl.multiple_of(tp * rows, rows), rows), :], wo[...])
    for cp in copies:
        cp.wait()
    for k in range(1, T):
        acc = acc + recvb[k - 1].astype(F32)
    for j in range(D // LANE):
        cols = slice(j * LANE, (j + 1) * LANE)
        out_ref[:, cols] = (tok_ref[:, cols].astype(F32) + vec(4, j) * acc[:, cols]).astype(BF16)


def local(
    latent_tokens, context_tokens, cond, ctx_cond, mod_shift, mod_scale, mod_gate, norm_gain,
    w_query, query_gain, w_down_kv, w_rope_key, kv_gain, w_up_kv, key_gain, ctx_lift, w_output,
):
    SP, T = lax.axis_size("sp"), lax.axis_size("tp")
    Y = C = 2
    Z = SP // (Y * C)
    rows, D = latent_tokens.shape
    crows = context_tokens.shape[0]
    heads = ctx_lift.shape[0]
    prows, pcols = mod_shift.shape
    kvl = w_down_kv.shape[1]
    q = -(-(5 * pcols // LANE) // SP)
    group = rows * T
    seq = group * SP
    n = seq + crows * SP
    crp = max(16, crows)
    inv = THETA ** (-np.arange(ROPE // 4, dtype=np.float64) / (ROPE // 4))
    pos = np.arange(seq)
    ang = np.concatenate([inv[:, None] * (pos // GRID_W), inv[:, None] * (pos % GRID_W)], axis=0)
    cos, sin = np.cos(ang).astype(np.float32), np.sin(ang).astype(np.float32)
    vm = pl.BlockSpec(memory_space=pltpu.VMEM)
    hbm = pl.BlockSpec(memory_space=pl.ANY)
    sm = pl.BlockSpec(memory_space=pltpu.SMEM)
    dma = pltpu.SemaphoreType.DMA
    V = pltpu.VMEM
    ND = SP * T
    return pl.pallas_call(
        functools.partial(kernel, (SP, T, Y, C, q, rows, crows, heads)),
        out_shape=jax.ShapeDtypeStruct((rows, D), BF16),
        in_specs=[vm] * 8 + [hbm, vm, hbm, hbm, vm, hbm, vm, sm, hbm, vm, vm],
        out_specs=vm,
        scratch_shapes=[
            V(w_query.shape, BF16), V(w_down_kv.shape, BF16), V(w_rope_key.shape, BF16),
            V(w_up_kv.shape, BF16), V(w_output.shape, BF16),
            V((SP, q, LANE), F32), V((SP, q, LANE), F32), V((q, LANE), F32), V((T, SP, q, LANE), F32),
            V((T, rows, D), BF16), V((T, rows, D), BF16), V((crows, D), BF16),
            V((Z, Y, C, T, rows + 16, kvl), BF16), V((Z, Y, C, crp + 16, kvl), BF16),
            V((n, kvl), BF16), V((ROPE, n), F32), V((1, n), F32), V((w_up_kv.shape[2], kvl), BF16),
            V((heads, group, QK), BF16), V((group, heads * HD), BF16),
            V((T - 1, rows, D), BF16), V((T - 1, rows, D), BF16),
            dma((5,)), dma((T - 1,)), dma((T - 1,)), dma((SP - 1,)), dma((SP - 1,)),
            dma((ND - 1,)), dma((ND - 1,)), dma((Z - 1,)), dma((Z - 1,)), dma((Z - 1,)), dma((Z - 1,)),
            dma((1,)), dma((1,)), dma((1,)), dma((1,)), dma((T - 1,)), dma((T - 1,)),
            dma((1,)), dma((1,)), dma((1,)), dma((1,)), dma((T - 1,)), dma((T - 1,)),
        ],
        compiler_params=pltpu.CompilerParams(
            collective_id=0, has_side_effects=True, vmem_limit_bytes=60 * 1024 * 1024),
    )(
        latent_tokens, context_tokens, cond.reshape(SP, prows), ctx_cond.reshape(SP, prows),
        mod_shift, mod_scale, mod_gate, norm_gain.reshape(1, -1), w_query, query_gain.reshape(1, -1),
        w_down_kv, w_rope_key, kv_gain.reshape(1, -1), w_up_kv, key_gain.reshape(1, -1), ctx_lift,
        w_output, cos, sin,
    )


def solution(mesh):
    return jax.shard_map(
        local,
        mesh=mesh,
        in_specs=(
            P(("sp", "tp"), None),
            P("sp", None),
            P(),
            P(),
            P("sp", "tp"),
            P("sp", "tp"),
            P("sp", "tp"),
            P(),
            P(None, "tp"),
            P(),
            P(),
            P(),
            P(),
            P(None, None, "tp"),
            P(),
            P("tp"),
            P("tp", None),
        ),
        out_specs=P(("sp", "tp"), None),
        check_vma=False,
    )
```

time: 200 us -> 59.6 us (0.30)
  blocking collectives: 117 us -> 0 us
  Pallas kernels: 0 us -> 55.9 us
  matrix products: 25.4 us -> 0 us
  other arithmetic: 18.4 us -> 0 us
  between operations: 13.6 us -> 0.01 us
  waiting for transfers between devices: 11.9 us -> 0 us
  local copies, waits for them, and re-layouts: 12.3 us -> 3.57 us
    all_gather x2 -> x0, blocking collectives: 74.9 us -> none  [the longest x1 66.9 us: local(): lax.all_gather(own_rope, ('sp', 'tp'), axis=0, tiled=True)]
    pallas_call x0 -> x1, Pallas kernels: none -> 55.9 us  [local(): pl.pallas_call(functools.partial(kernel, (SP, T, Y, C, q, rows, crows, he...]
    psum x1 -> x0, blocking collectives: 42.3 us -> none  [local(): lax.psum((widen(shift_part), widen(scale_part), widen(gate_part)), ('sp',...]
    dot_general x17 -> x0, matrix products: 25.4 us -> none  [the longest x2 4.84 us: absorb(): jnp.einsum('qhd,khd->hqk', query_heads, keys, preferred_element_type=jnp....]
    reduce_scatter x1 -> x0, waiting for transfers between devices: 11.1 us -> none  [local(): lax.psum_scatter(jnp.dot(attended, w_output, preferred_element_type=jnp.f...]
    reduce_sum x7 -> x0, other arithmetic: 6.52 us -> none  [the longest x5 4.24 us: rms_normed(): jnp.mean(values * values, axis=-1, keepdims=True) + EPS]
    convert_element_type x5 -> x0, other arithmetic: 4.16 us -> none  [the longest x1 1.73 us: local(): (latent_tokens.astype(jnp.float32) + gate_vec[0] * out).astype(jnp.bfloat16)]
    dot_general x2 -> x0, local copies, waits for them, and re-layouts: 3.45 us -> none  [expand(): jnp.dot(latent, w_up_kv[0], preferred_element_type=jnp.float32)]
  transfers between devices with their start and end apart: 3 -> 0, of which waited for: 1 -> 0; matrix products, arithmetic and copies ran while one was open for 14% -> 0% of each run, Pallas kernels for 0% -> 0%
where the time goes in v1:
time: 59.6 us; the launch traced here: 59.4 us
  Pallas kernels  55.9 us (94%)
  local copies, waits for them, and re-layouts  3.57 us (6%)
    pallas_call x1, Pallas kernels, local(): pl.pallas_call(functools.partial(kernel, (SP, T, Y, C, q, rows, crows, he...  55.9 us
    unnamed x2, local copies, waits for them, and re-layouts  3.57 us

profile of v1, /device:TPU:0, one launch (start us, length us, event | category | flops | bytes accessed | tf_op | source)
XLA Modules:
  0.0 59.4 jit_solution(9850992318731232133)
XLA Ops:
  0.0 1.9 %copy.20.wr_hbm = bf16[2048,32]{1,0:T(8,128)(2,1)} copy(bf16[2048,32]{0,1:T(8,128)(2,1)} %param.30) | data formatting | bytes 262144 | tf_op args[11]
  1.9 55.9 %shard_map.181 = bf16[64,2048]{1,0:T(8,128)(2,1)} custom-call(bf16[64,2048]{1,0:T(8,128)(2,1)} %tok_ref.1, bf16[32,2048]{1,0:T(8,128)(2,1)} %ctx_ref.1, f32[16,128]{1,0:T(8,128)} %bitcast.6, f32[16,128]{1,0:T(8,128)} %bitcast.7, bf16[128,1024]{1,0:T(8,128)(2,1)} %mshift_ref.1, bf16[128,1024]{1,0:T(8,128)(2,1)} %mscale_ref.1, bf16[128,1024]{1,0:T(8,128)(2,1)} %mgate_ref.1, ...), custom_call_target="tpu_custom_call" | custom-call | tf_op jit(solution)/shard_map/pallas_call | solution.py:363
  57.8 1.7 %copy.22 = bf16[64,2048]{1,0:T(8,128)(2,1)} copy(bf16[64,2048]{1,0:T(8,128)(2,1)} %shard_map.181) | data formatting | bytes 524288

commit v2 on v1

v2 whole, which is shorter than its diff:
```python
import functools

import jax
import jax.numpy as jnp
import numpy as np
from jax import lax
from jax.experimental import pallas as pl
from jax.experimental.pallas import tpu as pltpu
from jax.sharding import PartitionSpec as P

HD = 64
ROPE = 32
QK = 96
GRID_W = 64
EPS = 1e-06
THETA = 10000.0
LANE = 128
MESH = pl.DeviceIdType.MESH
F32 = jnp.float32
BF16 = jnp.bfloat16

NN = (((1,), (0,)), ((), ()))
NT = (((1,), (1,)), ((), ()))


def dot(a, b, dims=NN):
    return lax.dot_general(a, b, dims, preferred_element_type=F32)


def column(row):
    return jnp.transpose(jnp.broadcast_to(row, (LANE, row.shape[1])))


def kernel(
    sizes,
    tok_ref, ctx_ref, cond_ref, cctx_ref, mshift_hbm, mscale_hbm, mgate_hbm, ngain_ref,
    wq_hbm, qgain_ref, wd_hbm, wr_hbm, kvgain_ref, wup_hbm, kgain_ref, lift_ref, wo_hbm,
    cos_hbm, sin_hbm,
    out_hbm,
    mshift_ref, mscale_ref, mgate_ref, cos_ref, sin_ref, out_ref,
    wq, wd, wr, wup, wo, part, rsb, red, mod, tokall, hid, chid, G, H, X, rot, ssr, wkT, Q, att,
    sendb, recvb,
    wsem, osem, tok_s, tok_r, rs_s, rs_r, ag_s, ag_r, gz_s, gz_r, hz_s, hz_r, gy_s, gy_r, hy_s, hy_r,
    gx_s, gx_r, gc_s, gc_r, hc_s, hc_r, f2_s, f2_r, f3_s, f3_r, ob_s, ob_r,
):
    SP, T, Y, C, q, rows, crows, heads, split, chunks = sizes
    Z = SP // (Y * C)
    ND = SP * T
    D = tok_ref.shape[1]
    group = rows * T
    crp = H.shape[3] - 16
    n_ctx = crows * SP
    n_lat = group * SP
    N = n_ctx + n_lat
    sp = lax.axis_index("sp")
    tp = lax.axis_index("tp")
    c = lax.rem(sp, C)
    y = lax.rem(sp // C, Y)
    z = sp // (C * Y)
    flat = sp * T + tp

    barrier = pltpu.get_barrier_semaphore()

    def greet(k, _):
        other = lax.rem(flat + k, ND)
        pl.semaphore_signal(barrier, inc=1, device_id=(other // T, lax.rem(other, T)), device_id_type=MESH)
        return 0

    lax.fori_loop(1, ND, greet, 0)

    wcopies = [
        pltpu.make_async_copy(src, dst, wsem.at[i])
        for i, (src, dst) in enumerate((
            (mshift_hbm, mshift_ref), (mscale_hbm, mscale_ref), (mgate_hbm, mgate_ref), (wd_hbm, wd),
            (wr_hbm, wr), (wup_hbm, wup), (cos_hbm, cos_ref), (sin_hbm, sin_ref), (wq_hbm, wq), (wo_hbm, wo)))
    ]
    for cp in wcopies:
        cp.start()

    sig_l = cond_ref[pl.ds(sp, 1), :]
    sig_l = column(sig_l * jax.nn.sigmoid(sig_l))
    sig_c = cctx_ref[pl.ds(sp, 1), :]
    sig_c = column(sig_c * jax.nn.sigmoid(sig_c))
    pcols = mshift_ref.shape[1] // LANE
    for cp in wcopies[:3]:
        cp.wait()

    def put(v, j, val):
        i = v * pcols + j
        part[i // q, i % q : i % q + 1, :] = val

    for j in range(pcols):
        cols = slice(j * LANE, (j + 1) * LANE)
        w = mshift_ref[:, cols].astype(F32)
        put(0, j, jnp.sum(w * sig_l, axis=0, keepdims=True))
        put(1, j, jnp.sum(w * sig_c, axis=0, keepdims=True))
        w = mscale_ref[:, cols].astype(F32)
        put(2, j, jnp.sum(w * sig_l, axis=0, keepdims=True))
        put(3, j, jnp.sum(w * sig_c, axis=0, keepdims=True))
        w = mgate_ref[:, cols].astype(F32)
        put(4, j, jnp.sum(w * sig_l, axis=0, keepdims=True))
    for i in range(5 * pcols, SP * q):
        part[i // q, i % q : i % q + 1, :] = jnp.zeros((1, LANE), F32)

    pl.semaphore_wait(barrier, ND - 1)

    def rs_copy(k):
        other = lax.rem(sp + k, SP)
        return pltpu.make_async_remote_copy(
            src_ref=part.at[other], dst_ref=rsb.at[sp], send_sem=rs_s.at[k - 1], recv_sem=rs_r.at[k - 1],
            device_id=(other, tp), device_id_type=MESH)

    def rs_start(k, _):
        rs_copy(k).start()
        return 0

    lax.fori_loop(1, SP, rs_start, 0)

    def tp_copy(k, src, dst, s, r):
        return pltpu.make_async_remote_copy(
            src_ref=src, dst_ref=dst, send_sem=s.at[k - 1], recv_sem=r.at[k - 1],
            device_id=(sp, lax.rem(tp + k, T)), device_id_type=MESH)

    tok_copies = [tp_copy(k, tok_ref, tokall.at[tp], tok_s, tok_r) for k in range(1, T)]
    rsb[sp] = part[sp]

    def rs_wait(k, _):
        rs_copy(k).wait()
        return 0

    lax.fori_loop(1, SP, rs_wait, 0)
    total = rsb[0]
    for i in range(1, SP):
        total = total + rsb[i]
    red[...] = total

    def ag_copy(k):
        other = lax.rem(flat + k, ND)
        return pltpu.make_async_remote_copy(
            src_ref=red, dst_ref=mod.at[tp, sp], send_sem=ag_s.at[k - 1], recv_sem=ag_r.at[k - 1],
            device_id=(other // T, lax.rem(other, T)), device_id_type=MESH)

    def ag_start(k, _):
        ag_copy(k).start()
        return 0

    lax.fori_loop(1, ND, ag_start, 0)
    for cp in tok_copies:
        cp.start()
    mod[tp, sp] = total

    for cp in wcopies[3:6]:
        cp.wait()
    wkT[...] = jnp.transpose(wup[0].astype(F32)).astype(BF16)
    kg = column(kgain_ref[...])
    qg = column(qgain_ref[...])
    my_ctx = ctx_ref[pl.ds(pl.multiple_of(tp * 16, 16), 16), :] if split else ctx_ref[...]
    my_ctx = my_ctx.astype(F32)
    invc = lax.rsqrt(jnp.mean(my_ctx * my_ctx, axis=1, keepdims=True) + EPS)
    my_tok = tok_ref[...].astype(F32)
    invt = lax.rsqrt(jnp.mean(my_tok * my_tok, axis=1, keepdims=True) + EPS)

    def ag_wait(k, _):
        ag_copy(k).wait()
        return 0

    lax.fori_loop(1, ND, ag_wait, 0)

    def vec(v, col):
        i = v * pcols + col % pcols
        return mod[col // pcols, i // q, i % q : i % q + 1, :]

    def modulate(x, inv, j, a, b):
        cols = slice(j * LANE, (j + 1) * LANE)
        return (x[:, cols] * inv * ngain_ref[:, cols] * (1.0 + vec(a, j)) + vec(b, j)).astype(BF16)

    for j in range(D // LANE):
        cols = slice(j * LANE, (j + 1) * LANE)
        hid[tp, :, cols] = modulate(my_tok, invt, j, 2, 0)
        chid[:, cols] = modulate(my_ctx, invc, j, 3, 1)

    def squeeze(raw):
        return (raw * lax.rsqrt(jnp.mean(raw * raw, axis=1, keepdims=True) + EPS) * kvgain_ref[...]).astype(BF16)

    lane = lax.broadcasted_iota(jnp.int32, (ROPE, LANE), 1)
    own = hid[tp]
    own_c = chid[...]
    crn = own_c.shape[0]
    lrope = dot(wr[...], jnp.concatenate([own] * T, axis=0), NT)
    crope = dot(wr[...], jnp.concatenate([own_c.astype(F32)] * (LANE // crn), axis=0).astype(BF16), NT)
    llo = tp * rows
    lrope = jnp.where((lane >= llo) & (lane < llo + rows), lrope, 0.0)
    per = (rows if split else LANE) // crn
    clo = lax.rem(sp, per) * crn
    if split:
        clo = clo + lax.rem(tp + 1, T) * rows
    crope = jnp.where((lane >= clo) & (lane < clo + crn), crope, 0.0)
    if split:
        lrope = lrope + crope
        lats = squeeze(dot(jnp.concatenate([own, own_c], axis=0), wd[...]))
        G[z, y, c, tp, rows + 16 : rows + 32] = lats[rows:]
        G[z, y, c, tp, 0:rows] = lats[:rows]
    else:
        H[z, y, c, 0:crows] = squeeze(dot(own_c, wd[...]))
        H[z, y, c, crp : crp + 16] = jnp.concatenate([crope[:16], crope[16:]], axis=1).astype(BF16)
        G[z, y, c, tp, 0:rows] = squeeze(dot(own, wd[...]))
    G[z, y, c, tp, rows : rows + 16] = jnp.concatenate([lrope[:16], lrope[16:]], axis=1).astype(BF16)

    def at(zz, yy, cc):
        return (zz * Y + yy) * C + cc

    def remote(src, s, r, dev):
        return pltpu.make_async_remote_copy(
            src_ref=src, dst_ref=src, send_sem=s, recv_sem=r, device_id=dev, device_id_type=MESH)

    zc = []
    for k in range(1, Z):
        dev = (at(lax.rem(z + k, Z), y, c), tp)
        zc.append(remote(G.at[z, y, c, tp], gz_s.at[k - 1], gz_r.at[k - 1], dev))
        if not split:
            zc.append(remote(H.at[z, y, c], hz_s.at[k - 1], hz_r.at[k - 1], dev))
    for cp in zc:
        cp.start()

    for cp in tok_copies:
        cp.wait()
    for k in range(1, T):
        t = lax.rem(tp + k, T)
        x = tokall[t].astype(F32)
        inv = lax.rsqrt(jnp.mean(x * x, axis=1, keepdims=True) + EPS)
        for j in range(D // LANE):
            hid[t, :, j * LANE : (j + 1) * LANE] = modulate(x, inv, j, 2, 0)
    for cp in wcopies[6:9]:
        cp.wait()
    hid_all = hid[...].reshape(group, D)
    raw = dot(hid_all, wq[...])
    rawT = jnp.transpose(raw)
    cosg = cos_ref[:, pl.ds(pl.multiple_of(sp * group, group), group)]
    sing = sin_ref[:, pl.ds(pl.multiple_of(sp * group, group), group)]
    fold = QK ** (-0.5) * 1.4426950408889634
    for h in range(heads):
        u = rawT[h * QK : (h + 1) * QK]
        u = u * (lax.rsqrt(jnp.mean(u * u, axis=0, keepdims=True) + EPS) * fold) * qg[:, :group]
        f, b = u[HD : HD + 16], u[HD + 16 :]
        u = jnp.concatenate([u[:HD], f * cosg - b * sing, b * cosg + f * sing], axis=0)
        Q[h] = jnp.transpose(u).astype(BF16)

    for cp in zc:
        cp.wait()

    ydev = (at(z, Y - 1 - y, c), tp)
    cdev = (at(z, y, C - 1 - c), tp)

    def xdev(k):
        return (sp, lax.rem(tp + k, T))

    def start(copies):
        for cp in copies:
            cp.start()
        return copies

    def wait(copies):
        for cp in copies:
            cp.wait()

    def finish(sent, got):
        for cp in sent:
            cp.wait_send()
        for cp in got:
            cp.wait_recv()

    first = start([remote(G.at[:, y, c, tp], gc_s.at[0], gc_r.at[0], cdev)])
    others = [lax.rem(tp + k, T) for k in range(1, T)]

    def fwd2(cc):
        if cc == 0:
            return [remote(G.at[:, 1 - y, 0, tp], f2_s.at[0], f2_r.at[0], cdev)]
        return [remote(G.at[:, y, 1, t], f2_s.at[k], f2_r.at[k], cdev) for k, t in enumerate(others)]

    def fwd3(cc):
        if cc == 0:
            return [remote(G.at[:, :, 0, t], f3_s.at[k], f3_r.at[k], cdev) for k, t in enumerate(others)]
        return [remote(G.at[:, 1 - y, 1], f3_s.at[0], f3_r.at[0], cdev)]

    @pl.when(c == 0)
    def _():
        wait(start([remote(G.at[:, y, 0, tp], gy_s.at[0], gy_r.at[0], ydev)]))
        last = start([remote(G.at[:, :, 0, tp], gx_s.at[k - 1], gx_r.at[k - 1], xdev(k)) for k in range(1, T)])
        sent = start(fwd2(0))
        wait(last)
        finish(sent + start(fwd3(0)), fwd2(1) + fwd3(1))

    @pl.when(c != 0)
    def _():
        wait(start([remote(G.at[:, y, 1, tp], gx_s.at[k - 1], gx_r.at[k - 1], xdev(k)) for k in range(1, T)]))
        last = start([remote(G.at[:, y, 1], gy_s.at[0], gy_r.at[0], ydev)])
        sent = start(fwd2(1))
        wait(last)
        finish(sent + start(fwd3(1)), fwd2(0) + fwd3(0))

    wait(first)
    if not split:
        wait(start([remote(H.at[:, y, c], hy_s.at[0], hy_r.at[0], ydev)]))
        wait(start([remote(H.at[:, :, c], hc_s.at[0], hc_r.at[0], cdev)]))

    def where_is(s):
        return s // (Y * C), (s // C) % Y, s % C

    gk = kg[HD:]
    gf, gb = gk[:16], gk[16:]

    def place(cols, total, pos):
        f, b = total[:, :LANE], total[:, LANE:]
        ssr[:, cols] = jnp.sum(f * f + b * b, axis=0, keepdims=True)
        f, b = f * gf, b * gb
        if pos is not None:
            cs, sn = cos_ref[:, pos], sin_ref[:, pos]
            f, b = f * cs - b * sn, b * cs + f * sn
        rot[0:16, cols] = f
        rot[16:32, cols] = b

    lane2 = lax.rem(lax.broadcasted_iota(jnp.int32, (16, 2 * LANE), 1), LANE) // rows

    def mix(blocks):
        total = blocks[0]
        for t in range(1, T):
            total = jnp.where(lane2 == t, blocks[t], total)
        return total

    ctotal = 0.0
    for s in range(SP):
        w = where_is(s)
        lo = n_ctx + s * group
        for t in range(T):
            X[lo + t * rows : lo + (t + 1) * rows] = G[w[0], w[1], w[2], t, 0:rows]
        blocks = [G[w[0], w[1], w[2], t, rows : rows + 16].astype(F32) for t in range(T)]
        place(slice(lo, lo + group), mix(blocks), slice(s * group, (s + 1) * group))
        if split:
            base = s // per * group
            for t in range(T):
                lo = base + (t + 1) % T * rows + s % per * 16
                X[lo : lo + 16] = G[w[0], w[1], w[2], t, rows + 16 : rows + 32]
            ctotal = ctotal + mix([blocks[(t - 1) % T] for t in range(T)])
            if s % per == per - 1:
                place(slice(base, base + group), ctotal, None)
                ctotal = 0.0
    if not split:
        if crows % 16 == 0:
            for s in range(SP):
                w = where_is(s)
                X[s * crows : (s + 1) * crows] = H[w[0], w[1], w[2], 0:crows]
        else:
            X[0:n_ctx] = jnp.concatenate(
                [H[where_is(s)][0:16].astype(F32)[:crows] for s in range(SP)], axis=0).astype(BF16)
        for s0 in range(0, SP, per):
            total = sum(H[where_is(s)][crp : crp + 16].astype(F32) for s in range(s0, s0 + per))
            place(slice(s0 * crows, s0 * crows + LANE), total, None)

    gp = kg[:HD, :1]
    ones = jnp.ones((N, LANE), BF16)
    half = lax.broadcasted_iota(jnp.int32, (group, LANE), 1) < HD

    def pair(p, _):
        lo = pl.multiple_of(p * LANE, LANE)
        kT = dot(wkT[pl.ds(lo, LANE), :], X[...], NT)
        val = jnp.concatenate([dot(X[...], wup[1, :, pl.ds(lo, LANE)]).astype(BF16), ones], axis=1)
        res = []
        for i in range(2):
            kp = kT[i * HD : (i + 1) * HD]
            inv = lax.rsqrt((jnp.sum(kp * kp, axis=0, keepdims=True) + ssr[...]) * (1.0 / QK) + EPS)
            key = jnp.concatenate([kp * gp * inv, rot[...] * inv], axis=0).astype(BF16)
            w = jnp.exp2(dot(Q[2 * p + i], key)).astype(BF16)
            drop = jnp.exp(jnp.full((1, 2 * LANE), -lift_ref[2 * p + i], F32))
            o = dot(w[:, :n_ctx], val[:n_ctx]) + drop * dot(w[:, n_ctx:], val[n_ctx:])
            res.append(o[:, :LANE] / o[:, LANE:])
        att[:, pl.ds(lo, LANE)] = jnp.where(half, res[0], res[1]).astype(BF16)
        return 0

    lax.fori_loop(0, heads // 2, pair, 0)

    wcopies[9].wait()
    width = D // chunks
    copies = []
    for j in range(chunks):
        cols = slice(j * width, (j + 1) * width)
        for k in range(1, T):
            t = lax.rem(tp + k, T)
            a = att[pl.ds(pl.multiple_of(t * rows, rows), rows), :]
            sendb[k - 1, :, cols] = dot(a, wo[:, cols]).astype(BF16)
            cp = pltpu.make_async_remote_copy(
                src_ref=sendb.at[k - 1, :, cols], dst_ref=recvb.at[k - 1, :, cols],
                send_sem=ob_s.at[j, k - 1], recv_sem=ob_r.at[j, k - 1],
                device_id=xdev(k), device_id_type=MESH)
            cp.start()
            copies.append(cp)
    acc = dot(att[pl.ds(pl.multiple_of(tp * rows, rows), rows), :], wo[...])
    outs = []
    for j in range(chunks):
        for k in range(1, T):
            copies[j * (T - 1) + k - 1].wait()
        for i in range(j * width // LANE, (j + 1) * width // LANE):
            cols = slice(i * LANE, (i + 1) * LANE)
            o = acc[:, cols]
            for k in range(1, T):
                o = o + recvb[k - 1, :, cols].astype(F32)
            out_ref[:, cols] = (tok_ref[:, cols].astype(F32) + vec(4, i) * o).astype(BF16)
        cols = slice(j * width, (j + 1) * width)
        cp = pltpu.make_async_copy(out_ref.at[:, cols], out_hbm.at[:, cols], osem.at[j])
        cp.start()
        outs.append(cp)
    for cp in outs:
        cp.wait()


def local(
    latent_tokens, context_tokens, cond, ctx_cond, mod_shift, mod_scale, mod_gate, norm_gain,
    w_query, query_gain, w_down_kv, w_rope_key, kv_gain, w_up_kv, key_gain, ctx_lift, w_output,
):
    SP, T = lax.axis_size("sp"), lax.axis_size("tp")
    Y = C = 2
    Z = SP // (Y * C)
    rows, D = latent_tokens.shape
    crows = context_tokens.shape[0]
    heads = ctx_lift.shape[0]
    prows, pcols = mod_shift.shape
    kvl = w_down_kv.shape[1]
    q = -(-(5 * pcols // LANE) // SP)
    group = rows * T
    seq = group * SP
    n = seq + crows * SP
    split = crows == 16 * T
    crp = 16 if split else max(16, crows)
    chunks = 4
    inv = THETA ** (-np.arange(ROPE // 4, dtype=np.float64) / (ROPE // 4))
    pos = np.arange(seq)
    ang = np.concatenate([inv[:, None] * (pos // GRID_W), inv[:, None] * (pos % GRID_W)], axis=0)
    cos, sin = np.cos(ang).astype(np.float32), np.sin(ang).astype(np.float32)
    vm = pl.BlockSpec(memory_space=pltpu.VMEM)
    hbm = pl.BlockSpec(memory_space=pl.ANY)
    sm = pl.BlockSpec(memory_space=pltpu.SMEM)
    dma = pltpu.SemaphoreType.DMA
    V = pltpu.VMEM
    ND = SP * T
    return pl.pallas_call(
        functools.partial(kernel, (SP, T, Y, C, q, rows, crows, heads, split, chunks)),
        out_shape=jax.ShapeDtypeStruct((rows, D), BF16),
        in_specs=[vm] * 4 + [hbm] * 3 + [vm, hbm, vm, hbm, hbm, vm, hbm, vm, sm, hbm, hbm, hbm],
        out_specs=hbm,
        scratch_shapes=[
            V(mod_shift.shape, BF16), V(mod_shift.shape, BF16), V(mod_shift.shape, BF16),
            V(cos.shape, F32), V(cos.shape, F32), V((rows, D), BF16),
            V(w_query.shape, BF16), V(w_down_kv.shape, BF16), V(w_rope_key.shape[::-1], BF16),
            V(w_up_kv.shape, BF16), V(w_output.shape, BF16),
            V((SP, q, LANE), F32), V((SP, q, LANE), F32), V((q, LANE), F32), V((T, SP, q, LANE), F32),
            V((T, rows, D), BF16), V((T, rows, D), BF16), V((16 if split else crows, D), BF16),
            V((Z, Y, C, T, rows + (32 if split else 16), kvl), BF16), V((Z, Y, C, crp + 16, kvl), BF16),
            V((n, kvl), BF16), V((ROPE, n), F32), V((1, n), F32), V((w_up_kv.shape[2], kvl), BF16),
            V((heads, group, QK), BF16), V((group, heads * HD), BF16),
            V((T - 1, rows, D), BF16), V((T - 1, rows, D), BF16),
            dma((10,)), dma((chunks,)), dma((T - 1,)), dma((T - 1,)), dma((SP - 1,)), dma((SP - 1,)),
            dma((ND - 1,)), dma((ND - 1,)), dma((Z - 1,)), dma((Z - 1,)), dma((Z - 1,)), dma((Z - 1,)),
            dma((1,)), dma((1,)), dma((1,)), dma((1,)), dma((T - 1,)), dma((T - 1,)),
            dma((1,)), dma((1,)), dma((1,)), dma((1,)), dma((T - 1,)), dma((T - 1,)), dma((T - 1,)), dma((T - 1,)),
            dma((chunks, T - 1)), dma((chunks, T - 1)),
        ],
        compiler_params=pltpu.CompilerParams(
            collective_id=0, has_side_effects=True, vmem_limit_bytes=60 * 1024 * 1024),
    )(
        latent_tokens, context_tokens, cond.reshape(SP, prows), ctx_cond.reshape(SP, prows),
        mod_shift, mod_scale, mod_gate, norm_gain.reshape(1, -1), w_query, query_gain.reshape(1, -1),
        w_down_kv, w_rope_key.T, kv_gain.reshape(1, -1), w_up_kv, key_gain.reshape(1, -1), ctx_lift,
        w_output, cos, sin,
    )


def solution(mesh):
    return jax.shard_map(
        local,
        mesh=mesh,
        in_specs=(
            P(("sp", "tp"), None),
            P("sp", None),
            P(),
            P(),
            P("sp", "tp"),
            P("sp", "tp"),
            P("sp", "tp"),
            P(),
            P(None, "tp"),
            P(),
            P(),
            P(),
            P(),
            P(None, None, "tp"),
            P(),
            P("tp"),
            P("tp", None),
        ),
        out_specs=P(("sp", "tp"), None),
        check_vma=False,
    )
```

time: 59.6 us -> 55 us (0.923)
  Pallas kernels: 55.9 us -> 53.2 us
  local copies, waits for them, and re-layouts: 3.57 us -> 1.67 us
    pallas_call x1, Pallas kernels: 55.9 us -> 53.2 us  [local(): pl.pallas_call(functools.partial(kernel, (SP, T, Y, C, q, rows, crows, he...]
    unnamed x2 -> x1, local copies, waits for them, and re-layouts: 3.57 us -> 1.67 us
where the time goes in v2:
time: 55 us; the launch traced here: 54.9 us
  Pallas kernels  53.2 us (97%)
  local copies, waits for them, and re-layouts  1.67 us (3%)
    pallas_call x1, Pallas kernels, local(): pl.pallas_call(functools.partial(kernel, (SP, T, Y, C, q, rows, crows, he...  53.2 us
    unnamed x1, local copies, waits for them, and re-layouts  1.67 us

profile of v2, /device:TPU:0, one launch (start us, length us, event | category | flops | bytes accessed | tf_op | source)
XLA Modules:
  0.0 54.9 jit_solution(7760826307733570816)
XLA Ops:
  0.0 53.2 %shard_map.181 = bf16[64,2048]{1,0:T(8,128)(2,1)} custom-call(bf16[64,2048]{1,0:T(8,128)(2,1)} %tok_ref.1, bf16[32,2048]{1,0:T(8,128)(2,1)} %ctx_ref.1, f32[16,128]{1,0:T(8,128)} %bitcast.8, f32[16,128]{1,0:T(8,128)} %bitcast.9, bf16[128,1024]{1,0:T(8,128)(2,1)} %mshift_hbm.1, bf16[128,1024]{1,0:T(8,128)(2,1)} %mscale_hbm.1, bf16[128,1024]{1,0:T(8,128)(2,1)} %mgate_hbm.1, ...), custom_call_target="tpu_custom_call" | custom-call | tf_op jit(solution)/shard_map/pallas_call | solution.py:444
  53.2 1.7 %copy.21 = bf16[64,2048]{1,0:T(8,128)(2,1)} copy(bf16[64,2048]{1,0:T(8,128)(2,1)} %shard_map.181) | data formatting | bytes 524288

commit v3 on v2

--- a/solution.py
+++ b/solution.py
@@ -41,7 +41,7 @@
     wq, wd, wr, wup, wo, part, rsb, red, mod, tokall, hid, chid, G, H, X, rot, ssr, wkT, Q, att,
     sendb, recvb,
     wsem, osem, tok_s, tok_r, rs_s, rs_r, ag_s, ag_r, gz_s, gz_r, hz_s, hz_r, gy_s, gy_r, hy_s, hy_r,
-    gx_s, gx_r, gc_s, gc_r, hc_s, hc_r, f2_s, f2_r, f3_s, f3_r, ob_s, ob_r,
+    gx_s, gx_r, rl_s, rl_r, gc_s, gc_r, hc_s, hc_r, f2_s, f2_r, f3_s, f3_r, ob_s, ob_r,
 ):
     SP, T, Y, C, q, rows, crows, heads, split, chunks = sizes
     Z = SP // (Y * C)
@@ -213,14 +213,48 @@
         return pltpu.make_async_remote_copy(
             src_ref=src, dst_ref=src, send_sem=s, recv_sem=r, device_id=dev, device_id_type=MESH)
 
-    zc = []
+    ydev = (at(z, Y - 1 - y, c), tp)
+    cdev = (at(z, y, C - 1 - c), tp)
+
+    def xdev(k):
+        return (sp, lax.rem(tp + k, T))
+
+    def start(copies):
+        for cp in copies:
+            cp.start()
+        return copies
+
+    def wait(copies):
+        for cp in copies:
+            cp.wait()
+
+    def finish(sent, got):
+        for cp in sent:
+            cp.wait_send()
+        for cp in got:
+            cp.wait_recv()
+
+    zs = [lax.rem(z - k + Z, Z) for k in range(Z)]
+    zc, hc = [], []
     for k in range(1, Z):
         dev = (at(lax.rem(z + k, Z), y, c), tp)
         zc.append(remote(G.at[z, y, c, tp], gz_s.at[k - 1], gz_r.at[k - 1], dev))
         if not split:
-            zc.append(remote(H.at[z, y, c], hz_s.at[k - 1], hz_r.at[k - 1], dev))
-    for cp in zc:
+            hc.append(remote(H.at[z, y, c], hz_s.at[k - 1], hz_r.at[k - 1], dev))
+    for cp in zc + hc:
         cp.start()
+
+    def ycol(zz):
+        return remote(G.at[zz, y, c, tp], gy_s.at[zz], gy_r.at[zz], ydev)
+
+    def xcol(k, zz):
+        return remote(G.at[zz, y, c, tp], gx_s.at[k - 1, zz], gx_r.at[k - 1, zz], xdev(k))
+
+    def got(ref, s, sem):
+        return pltpu.make_async_remote_copy(
+            src_ref=ref, dst_ref=ref, send_sem=s, recv_sem=sem, device_id=ydev, device_id_type=MESH)
+
+    column_copies = start([ycol(zs[0])] + [xcol(k, zs[0]) for k in range(1, T)])
 
     for cp in tok_copies:
         cp.wait()
@@ -245,29 +279,11 @@
         u = jnp.concatenate([u[:HD], f * cosg - b * sing, b * cosg + f * sing], axis=0)
         Q[h] = jnp.transpose(u).astype(BF16)
 
-    for cp in zc:
+    for k in range(1, Z):
+        zc[k - 1].wait()
+        column_copies += start([ycol(zs[k])] + [xcol(j, zs[k]) for j in range(1, T)])
+    for cp in hc:
         cp.wait()
-
-    ydev = (at(z, Y - 1 - y, c), tp)
-    cdev = (at(z, y, C - 1 - c), tp)
-
-    def xdev(k):
-        return (sp, lax.rem(tp + k, T))
-
-    def start(copies):
-        for cp in copies:
-            cp.start()
-        return copies
-
-    def wait(copies):
-        for cp in copies:
-            cp.wait()
-
-    def finish(sent, got):
-        for cp in sent:
-            cp.wait_send()
-        for cp in got:
-            cp.wait_recv()
 
     first = start([remote(G.at[:, y, c, tp], gc_s.at[0], gc_r.at[0], cdev)])
     others = [lax.rem(tp + k, T) for k in range(1, T)]
@@ -282,22 +298,42 @@
             return [remote(G.at[:, :, 0, t], f3_s.at[k], f3_r.at[k], cdev) for k, t in enumerate(others)]
         return [remote(G.at[:, 1 - y, 1], f3_s.at[0], f3_r.at[0], cdev)]
 
+    def y_in(zz):
+        return got(G.at[zz, 1 - y, c, tp], gy_s.at[zz], gy_r.at[zz])
+
+    def x_in(k, zz):
+        return got(G.at[zz, y, c, lax.rem(tp - k + T, T)], gx_s.at[k - 1, zz], gx_r.at[k - 1, zz])
+
     @pl.when(c == 0)
     def _():
-        wait(start([remote(G.at[:, y, 0, tp], gy_s.at[0], gy_r.at[0], ydev)]))
-        last = start([remote(G.at[:, :, 0, tp], gx_s.at[k - 1], gx_r.at[k - 1], xdev(k)) for k in range(1, T)])
+        relayed = []
+        for zz in zs:
+            y_in(zz).wait_recv()
+            relayed += start([
+                remote(G.at[zz, 1 - y, 0, tp], rl_s.at[k - 1, zz], rl_r.at[k - 1, zz], xdev(k)) for k in range(1, T)])
         sent = start(fwd2(0))
-        wait(last)
+        for zz in zs:
+            for k in range(1, T):
+                x_in(k, zz).wait_recv()
+        wait(relayed)
         finish(sent + start(fwd3(0)), fwd2(1) + fwd3(1))
 
     @pl.when(c != 0)
     def _():
-        wait(start([remote(G.at[:, y, 1, tp], gx_s.at[k - 1], gx_r.at[k - 1], xdev(k)) for k in range(1, T)]))
-        last = start([remote(G.at[:, y, 1], gy_s.at[0], gy_r.at[0], ydev)])
+        relayed = []
+        for zz in zs:
+            for k in range(1, T):
+                x_in(k, zz).wait_recv()
+                relayed += start([
+                    remote(G.at[zz, y, 1, lax.rem(tp - k + T, T)], rl_s.at[k - 1, zz], rl_r.at[k - 1, zz], ydev)])
         sent = start(fwd2(1))
-        wait(last)
+        for zz in zs:
+            y_in(zz).wait_recv()
+        wait(relayed)
         finish(sent + start(fwd3(1)), fwd2(0) + fwd3(0))
 
+    for cp in column_copies:
+        cp.wait_send()
     wait(first)
     if not split:
         wait(start([remote(H.at[:, y, c], hy_s.at[0], hy_r.at[0], ydev)]))
@@ -459,7 +495,7 @@
             V((T - 1, rows, D), BF16), V((T - 1, rows, D), BF16),
             dma((10,)), dma((chunks,)), dma((T - 1,)), dma((T - 1,)), dma((SP - 1,)), dma((SP - 1,)),
             dma((ND - 1,)), dma((ND - 1,)), dma((Z - 1,)), dma((Z - 1,)), dma((Z - 1,)), dma((Z - 1,)),
-            dma((1,)), dma((1,)), dma((1,)), dma((1,)), dma((T - 1,)), dma((T - 1,)),
+            dma((Z,)), dma((Z,)), dma((1,)), dma((1,)), dma((T - 1, Z)), dma((T - 1, Z)), dma((T - 1, Z)), dma((T - 1, Z)),
             dma((1,)), dma((1,)), dma((1,)), dma((1,)), dma((T - 1,)), dma((T - 1,)), dma((T - 1,)), dma((T - 1,)),
             dma((chunks, T - 1)), dma((chunks, T - 1)),
         ],

time: 55 us -> 51.2 us (0.931)
  Pallas kernels: 53.2 us -> 49.4 us
    pallas_call x1, Pallas kernels: 53.2 us -> 49.4 us  [local(): pl.pallas_call(functools.partial(kernel, (SP, T, Y, C, q, rows, crows, he...]
where the time goes in v3:
time: 51.2 us; the launch traced here: 51 us
  Pallas kernels  49.4 us (96%)
  local copies, waits for them, and re-layouts  1.67 us (3%)
    pallas_call x1, Pallas kernels, local(): pl.pallas_call(functools.partial(kernel, (SP, T, Y, C, q, rows, crows, he...  49.4 us
    unnamed x1, local copies, waits for them, and re-layouts  1.67 us

profile of v3, /device:TPU:0, one launch (start us, length us, event | category | flops | bytes accessed | tf_op | source)
XLA Modules:
  0.0 51.0 jit_solution(311890433770800258)
XLA Ops:
  0.0 49.4 %shard_map.181 = bf16[64,2048]{1,0:T(8,128)(2,1)} custom-call(bf16[64,2048]{1,0:T(8,128)(2,1)} %tok_ref.1, bf16[32,2048]{1,0:T(8,128)(2,1)} %ctx_ref.1, f32[16,128]{1,0:T(8,128)} %bitcast.8, f32[16,128]{1,0:T(8,128)} %bitcast.9, bf16[128,1024]{1,0:T(8,128)(2,1)} %mshift_hbm.1, bf16[128,1024]{1,0:T(8,128)(2,1)} %mscale_hbm.1, bf16[128,1024]{1,0:T(8,128)(2,1)} %mgate_hbm.1, ...), custom_call_target="tpu_custom_call" | custom-call | tf_op jit(solution)/shard_map/pallas_call | solution.py:480
  49.4 1.7 %copy.21 = bf16[64,2048]{1,0:T(8,128)(2,1)} copy(bf16[64,2048]{1,0:T(8,128)(2,1)} %shard_map.181) | data formatting | bytes 524288
